TPU v7x, 32 devices: a whole 2x2x4 slice. The times are simulated.
32 devices in a mesh: ep: 8 (over z, x), tp: 4 (over y, core).
Axes of the slice: x: 2, y: 2, z: 4, core: 2. Of those that a mesh axis runs over, the one named last changes fastest.
Arguments:
- stream: bfloat16 [2048, 3072], P('ep'), may hold values from -30 to 30
- ffn_gain: bfloat16 [3072], replicated, may hold values from 0.099609375 to 1.8984375
- chosen: int32 [8, 256], replicated, may hold values from 0 to 2047, as said below
- affinity: float32 [8, 256], P('ep'), may hold values from 0.5 to 2
- w_gate: bfloat16 [8, 3072, 3072], P('ep', None, 'tp'), may hold values from -0.109375 to 0.109375
- w_up: bfloat16 [8, 3072, 3072], P('ep', None, 'tp'), may hold values from -0.109375 to 0.109375
- w_down: bfloat16 [8, 3072, 3072], P('ep', 'tp'), may hold values from -0.109375 to 0.109375
- final_gain: bfloat16 [3072], P('tp'), may hold values from 0.099609375 to 1.8984375
Outputs:
- normed: bfloat16 [2048, 3072], P('ep', 'tp')
Inputs may be any that keep to these rules, and one draw needn't show every extreme that they name: `chosen`: row e holds 256 distinct token numbers in ascending order. Of the 256 tokens of one index of ep, each expert reads at least one and at most 48; in every draw some expert reads exactly 48 from some index.
All inputs are finite; a program needn't handle non-finite values.
Results may differ from a plain program's by a relative error of at most 0.015.
Values may be sent and summed in bfloat16 or wider, within the bound.
A program may use at most 128 MiB of HBM per device.

v0:
```python
import functools

import jax
import jax.numpy as jnp
from jax import lax
from jax.experimental import pallas as pl
from jax.experimental.pallas import tpu as pltpu
from jax.sharding import PartitionSpec as P

EPSILON = 1e-06
F32 = jnp.float32
BF16 = jnp.bfloat16
MESH = pl.DeviceIdType.MESH


def layer(
    experts, tp, chunks, slots,
    stream_hbm, gain_ref, chosen_ref, aff_ref, wg_hbm, wu_hbm, wd_hbm, fgain_ref,
    out_ref,
    x_v, xn_v, wg_v, wu_v, wd_v, sel_v, place_v, pack_v, spread_v, aff_v,
    send_v, recv_v, piece_v, accg_v, accu_v, hidden_v,
    psend_v, pown_v, prec_v, ysend_v, yrec_v, leave_v, ret_v, merged_v, ssq_v, gain_v,
    x_sem, w_sem, wd_sem,
    dsend, drecv, gsend, grecv, fsend, frecv, psend, precv, ysend, yrecv,
    rsend, rrecv, qsend, qrecv,
):
    me = lax.axis_index("ep")
    col = lax.axis_index("tp")
    tok = x_v.shape[0]
    width = x_v.shape[1]
    share = xn_v.shape[1]
    caps = chosen_ref.shape[1]
    cw = share // chunks
    rows = experts * slots
    chips = tp // 2
    y = col // 2
    core = col % 2
    partner = y * 2 + 1 - core

    barrier = pltpu.get_barrier_semaphore()
    for r in range(1, experts):
        pl.semaphore_signal(barrier, inc=1, device_id={"ep": (me + r) % experts}, device_id_type=MESH)
    for r in range(1, tp):
        pl.semaphore_signal(barrier, inc=1, device_id={"tp": (col + r) % tp}, device_id_type=MESH)

    x_copy = pltpu.make_async_copy(stream_hbm, x_v, x_sem)
    x_copy.start()
    w_copies = []
    for k in range(chunks):
        group = []
        for n, (src, dst) in enumerate(((wg_hbm, wg_v), (wu_hbm, wu_v))):
            for j in range(tp):
                copy = pltpu.make_async_copy(
                    src.at[pl.ds(j * share + k * cw, cw), :],
                    dst.at[k, pl.ds(j * cw, cw), :],
                    w_sem.at[k, n, j],
                )
                copy.start()
                group.append(copy)
        w_copies.append(group)
    wd_copy = pltpu.make_async_copy(wd_hbm, wd_v, wd_sem)
    wd_copy.start()

    base = (me * tok).astype(F32)
    lane_cap = lax.broadcasted_iota(jnp.int32, (slots, caps), 1).astype(F32)
    sub_slot = lax.broadcasted_iota(jnp.int32, (slots, caps), 0).astype(F32)
    lane_tok = lax.broadcasted_iota(jnp.int32, (slots, tok), 1).astype(F32)

    def build_sel(e, carry):
        row = chosen_ref[pl.ds(e, 1), :].astype(F32)
        start = jnp.sum(jnp.where(row < base, 1.0, 0.0), axis=1, keepdims=True)
        hit = lane_cap == sub_slot + start
        token = jnp.sum(jnp.where(hit, row + 1.0, 0.0), axis=1, keepdims=True) - 1.0 - base
        sel_v[e] = jnp.where(token == lane_tok, 1.0, 0.0).astype(BF16)
        return carry

    lax.fori_loop(0, experts, build_sel, 0)

    x_copy.wait()
    gain_v[...] = gain_ref[...].astype(F32)
    lines = share // 128
    gain = jnp.concatenate(
        [gain_v[pl.ds(col * lines + i, 1), :] for i in range(lines)], axis=1
    )
    step_rows = 16

    def norm_rows(i, carry):
        at = pl.ds(pl.multiple_of(i * step_rows, step_rows), step_rows)
        block = x_v[at, :].astype(F32)
        scale = lax.rsqrt(jnp.sum(block * block, axis=1, keepdims=True) / width + EPSILON)
        own = x_v[at, pl.ds(pl.multiple_of(col * share, 128), share)].astype(F32)
        xn_v[at, :] = (own * scale * gain).astype(BF16)
        return carry

    lax.fori_loop(0, tok // step_rows, norm_rows, 0)

    sel = sel_v[...].reshape(rows, tok)
    finish = []

    def exchange(k, src, dst, ssem, rsem):
        for r in range(1, experts):
            to = (me + r) % experts
            copy = pltpu.make_async_remote_copy(
                src_ref=src.at[k, to], dst_ref=dst.at[k, me],
                send_sem=ssem.at[k, r], recv_sem=rsem.at[k, r],
                device_id={"ep": to}, device_id_type=MESH,
            )
            copy.start()
            finish.append(copy)
        dst[k, me] = src[k, me]

    def exchange_wait(k, src, dst, ssem, rsem):
        for r in range(1, experts):
            frm = (me + experts - r) % experts
            pltpu.make_async_remote_copy(
                src_ref=src.at[k, me], dst_ref=dst.at[k, frm],
                send_sem=ssem.at[k, r], recv_sem=rsem.at[k, r],
                device_id={"ep": frm}, device_id_type=MESH,
            ).wait_recv()

    for k in range(chunks):
        out = jnp.dot(sel, xn_v[:, k * cw:(k + 1) * cw], preferred_element_type=F32)
        send_v[k] = out.astype(BF16).reshape(experts, slots, cw)
    pl.semaphore_wait(barrier, experts - 1 + tp - 1)
    for k in range(chunks):
        exchange(k, send_v, recv_v, dsend, drecv)

    own_row = chosen_ref[pl.ds(me, 1), :].astype(F32)
    lane_j = lax.broadcasted_iota(jnp.int32, (1, rows), 1).astype(F32)
    start_j = jnp.zeros((1, rows), F32)
    end_j = jnp.zeros((1, rows), F32)
    slot_j = lane_j
    start_d = jnp.zeros((1, 1), F32)
    for d in range(experts):
        end_d = jnp.sum(jnp.where(own_row < float((d + 1) * tok), 1.0, 0.0), axis=1, keepdims=True)
        mine = (lane_j >= float(d * slots)) & (lane_j < float((d + 1) * slots))
        start_j = start_j + jnp.where(mine, start_d, 0.0)
        end_j = end_j + jnp.where(mine, end_d, 0.0)
        slot_j = slot_j - jnp.where(mine, float(d * slots), 0.0)
        spread_v[d] = jnp.where(
            (lane_cap == sub_slot + start_d) & (lane_cap < end_d), 1.0, 0.0
        ).astype(BF16)
        start_d = end_d
    want = start_j + slot_j
    part = 32

    def build_pack(i, carry):
        at = pl.multiple_of(i * part, part)
        pick = (lax.broadcasted_iota(jnp.int32, (part, rows), 0) + at).astype(F32)
        pack_v[pl.ds(at, part), :] = jnp.where((pick == want) & (pick < end_j), 1.0, 0.0).astype(BF16)
        return carry

    lax.fori_loop(0, caps // part, build_pack, 0)

    square = 128
    eye = (
        lax.broadcasted_iota(jnp.int32, (square, square), 0)
        == lax.broadcasted_iota(jnp.int32, (square, square), 1)
    )
    for b in range(caps // square):
        weights = aff_ref[:, b * square:(b + 1) * square]
        aff_v[b * square:(b + 1) * square, :] = jnp.sum(
            jnp.where(eye, weights, 0.0), axis=1, keepdims=True
        )
    for b in range(rows // square):
        block = sel.astype(F32)[b * square:(b + 1) * square, :]
        place_v[:, b * square:(b + 1) * square] = block.T.astype(BF16)

    def part_of(k, j):
        return piece_v.at[k, :, pl.ds(pl.multiple_of(j * cw, 128), cw)]

    def gather_start(k):
        exchange_wait(k, send_v, recv_v, dsend, drecv)
        got = recv_v[k].reshape(rows, cw)
        own = jnp.dot(pack_v[...], got, preferred_element_type=F32).astype(BF16)
        piece_v[k, :, pl.ds(pl.multiple_of(col * cw, 128), cw)] = own
        for r in range(1, chips):
            to = ((y + r) % chips) * 2 + core
            copy = pltpu.make_async_remote_copy(
                src_ref=part_of(k, col), dst_ref=part_of(k, col),
                send_sem=gsend.at[k, r], recv_sem=grecv.at[k, r],
                device_id={"tp": to}, device_id_type=MESH,
            )
            copy.start()
            finish.append(copy)
        copy = pltpu.make_async_remote_copy(
            src_ref=part_of(k, col), dst_ref=part_of(k, col),
            send_sem=fsend.at[k, 0], recv_sem=frecv.at[k, 0],
            device_id={"tp": partner}, device_id_type=MESH,
        )
        copy.start()
        finish.append(copy)

    def gather_finish(k):
        for r in range(1, chips):
            frm = ((y + chips - r) % chips) * 2 + core
            pltpu.make_async_remote_copy(
                src_ref=part_of(k, col), dst_ref=part_of(k, frm),
                send_sem=gsend.at[k, r], recv_sem=grecv.at[k, r],
                device_id={"tp": frm}, device_id_type=MESH,
            ).wait_recv()
            copy = pltpu.make_async_remote_copy(
                src_ref=part_of(k, frm), dst_ref=part_of(k, frm),
                send_sem=fsend.at[k, r], recv_sem=frecv.at[k, r],
                device_id={"tp": partner}, device_id_type=MESH,
            )
            copy.start()
            finish.append(copy)
        for copy in w_copies[k]:
            copy.wait()
        for r in range(chips):
            theirs = ((y + chips - r) % chips) * 2 + 1 - core
            pltpu.make_async_remote_copy(
                src_ref=part_of(k, col), dst_ref=part_of(k, theirs),
                send_sem=fsend.at[k, r], recv_sem=frecv.at[k, r],
                device_id={"tp": partner}, device_id_type=MESH,
            ).wait_recv()
        taken = piece_v[k]
        gate = jnp.dot(taken, wg_v[k], preferred_element_type=F32)
        accg_v[...] = gate if k == 0 else accg_v[...] + gate
        up = jnp.dot(taken, wu_v[k], preferred_element_type=F32)
        accu_v[...] = up if k == 0 else accu_v[...] + up

    for k in range(chunks):
        gather_start(k)
        if k > 0:
            gather_finish(k - 1)
    gather_finish(chunks - 1)

    hblock = 32

    def activate(i, carry):
        at = pl.ds(pl.multiple_of(i * hblock, hblock), hblock)
        gate = accg_v[at, :]
        hidden_v[at, :] = (gate / (1.0 + jnp.exp(-gate)) * accu_v[at, :]).astype(BF16)
        return carry

    lax.fori_loop(0, caps // hblock, activate, 0)
    wd_copy.wait()

    def down(k, j):
        at = pl.ds(pl.multiple_of(j * share + k * cw, 128), cw)
        return jnp.dot(hidden_v[...], wd_v[:, at], preferred_element_type=F32)

    def pair_copy(k, r):
        return pltpu.make_async_remote_copy(
            src_ref=psend_v.at[k, r], dst_ref=prec_v.at[k, r],
            send_sem=psend.at[k, r], recv_sem=precv.at[k, r],
            device_id={"tp": partner}, device_id_type=MESH,
        )

    away = list(range(1, chips))

    def stage_pair(k, turns):
        for r in turns:
            to = (y + r) % chips
            psend_v[k, r] = down(k, to * 2 + 1 - core).astype(BF16)
            copy = pair_copy(k, r)
            copy.start()
            finish.append(copy)
        for r in turns:
            to = (y + r) % chips
            pown_v[k, r] = down(k, to * 2 + core)

    def chip_copy(k, r):
        to = ((y + r) % chips) * 2 + core
        return pltpu.make_async_remote_copy(
            src_ref=ysend_v.at[k, r], dst_ref=yrec_v.at[k, r],
            send_sem=ysend.at[k, r], recv_sem=yrecv.at[k, r],
            device_id={"tp": to}, device_id_type=MESH,
        )

    def stage_chip(k, turns):
        for r in turns:
            pair_copy(k, r).wait_recv()
            both = pown_v[k, r] + prec_v[k, r].astype(F32)
            if r == 0:
                pown_v[k, r] = both
            else:
                ysend_v[k, r] = both.astype(BF16)
                copy = chip_copy(k, r)
                copy.start()
                finish.append(copy)

    def stage_leave(k):
        total = pown_v[k, 0]
        for r in range(1, chips):
            chip_copy(k, r).wait_recv()
            total = total + yrec_v[k, r].astype(F32)
        weighted = (total * aff_v[...]).astype(BF16)
        spread = spread_v[...].reshape(rows, caps)
        out = jnp.dot(spread, weighted, preferred_element_type=F32)
        leave_v[k] = out.astype(BF16).reshape(experts, slots, cw)
        exchange(k, leave_v, ret_v, rsend, rrecv)

    for k in range(chunks):
        stage_pair(k, away)
        if k > 0:
            stage_chip(k - 1, away)
    stage_pair(0, [0])
    stage_chip(chunks - 1, away)
    for k in range(1, chunks):
        stage_pair(k, [0])
    for k in range(chunks):
        stage_chip(k, [0])
        stage_leave(k)

    squares = jnp.zeros((tok, 1), F32)
    for k in range(chunks):
        exchange_wait(k, leave_v, ret_v, rsend, rrecv)
        update = jnp.dot(place_v[...], ret_v[k].reshape(rows, cw), preferred_element_type=F32)
        at = pl.ds(pl.multiple_of(col * share + k * cw, 128), cw)
        merged = x_v[:, at].astype(F32) + update
        merged_v[:, k * cw:(k + 1) * cw] = merged
        squares = squares + jnp.sum(merged * merged, axis=1, keepdims=True)

    for b in range(tok // square):
        line = jnp.sum(
            jnp.where(eye, squares[b * square:(b + 1) * square, :], 0.0), axis=0, keepdims=True
        )
        ssq_v[0, :, b * square:(b + 1) * square] = jnp.broadcast_to(line, (8, square))

    def square_copy(r):
        return pltpu.make_async_remote_copy(
            src_ref=ssq_v.at[0], dst_ref=ssq_v.at[r],
            send_sem=qsend.at[r], recv_sem=qrecv.at[r],
            device_id={"tp": (col + r) % tp}, device_id_type=MESH,
        )

    for r in range(1, tp):
        copy = square_copy(r)
        copy.start()
        finish.append(copy)
    closing = fgain_ref[...].astype(F32)
    fgain = jnp.concatenate([closing[i:i + 1, :] for i in range(lines)], axis=1)
    sums = ssq_v[0]
    for r in range(1, tp):
        square_copy(r).wait_recv()
        sums = sums + ssq_v[r]
    for b in range(tok // square):
        line = sums[0:1, b * square:(b + 1) * square]
        column = jnp.sum(jnp.where(eye, line, 0.0), axis=1, keepdims=True)
        scale = lax.rsqrt(column / width + EPSILON)
        at = slice(b * square, (b + 1) * square)
        out_ref[at, :] = (merged_v[at, :] * scale * fgain).astype(BF16)

    for copy in finish:
        copy.wait_send()


def on_device(stream, ffn_gain, chosen, affinity, w_gate, w_up, w_down, final_gain):
    tok, width = stream.shape
    experts, caps = chosen.shape
    tp = lax.axis_size("tp")
    share = width // tp
    hid = w_gate.shape[2]
    slots = 3 * tok // 16
    chunks = 3 if share % 384 == 0 else 1
    cw = share // chunks
    chips = tp // 2
    rows = experts * slots
    vmem = pl.BlockSpec(memory_space=pltpu.VMEM)
    hbm = pl.BlockSpec(memory_space=pltpu.HBM)
    dma = pltpu.SemaphoreType.DMA
    buffers = [
        pltpu.VMEM((tok, width), BF16),
        pltpu.VMEM((tok, share), BF16),
        pltpu.VMEM((chunks, tp * cw, hid), BF16),
        pltpu.VMEM((chunks, tp * cw, hid), BF16),
        pltpu.VMEM((hid, width), BF16),
        pltpu.VMEM((experts, slots, tok), BF16),
        pltpu.VMEM((tok, rows), BF16),
        pltpu.VMEM((caps, rows), BF16),
        pltpu.VMEM((experts, slots, caps), BF16),
        pltpu.VMEM((caps, 1), F32),
        pltpu.VMEM((chunks, experts, slots, cw), BF16),
        pltpu.VMEM((chunks, experts, slots, cw), BF16),
        pltpu.VMEM((chunks, caps, tp * cw), BF16),
        pltpu.VMEM((caps, hid), F32),
        pltpu.VMEM((caps, hid), F32),
        pltpu.VMEM((caps, hid), BF16),
        pltpu.VMEM((chunks, chips, caps, cw), BF16),
        pltpu.VMEM((chunks, chips, caps, cw), F32),
        pltpu.VMEM((chunks, chips, caps, cw), BF16),
        pltpu.VMEM((chunks, chips, caps, cw), BF16),
        pltpu.VMEM((chunks, chips, caps, cw), BF16),
        pltpu.VMEM((chunks, experts, slots, cw), BF16),
        pltpu.VMEM((chunks, experts, slots, cw), BF16),
        pltpu.VMEM((tok, share), F32),
        pltpu.VMEM((tp, 8, tok), F32),
        pltpu.VMEM((width // 128, 128), F32),
    ]
    return pl.pallas_call(
        functools.partial(layer, experts, tp, chunks, slots),
        out_shape=jax.ShapeDtypeStruct((tok, share), BF16),
        in_specs=[hbm, vmem, vmem, vmem, hbm, hbm, hbm, vmem],
        out_specs=vmem,
        scratch_shapes=buffers + [
            dma, dma((chunks, 2, tp)), dma,
            dma((chunks, experts)), dma((chunks, experts)),
            dma((chunks, chips)), dma((chunks, chips)),
            dma((chunks, chips)), dma((chunks, chips)),
            dma((chunks, chips)), dma((chunks, chips)),
            dma((chunks, chips)), dma((chunks, chips)),
            dma((chunks, experts)), dma((chunks, experts)),
            dma((tp,)), dma((tp,)),
        ],
        compiler_params=pltpu.CompilerParams(
            collective_id=0, has_side_effects=True, vmem_limit_bytes=60 * 1024 * 1024
        ),
        name="layer",
    )(
        stream,
        ffn_gain.reshape(width // 128, 128),
        chosen,
        affinity,
        w_gate[0],
        w_up[0],
        w_down[0],
        final_gain.reshape(share // 128, 128),
    )


def solution(mesh):
    return jax.shard_map(
        on_device,
        mesh=mesh,
        in_specs=(
            P("ep", None),
            P(),
            P(),
            P("ep", None),
            P("ep", None, "tp"),
            P("ep", None, "tp"),
            P("ep", "tp", None),
            P("tp"),
        ),
        out_specs=P("ep", "tp"),
        check_vma=False,
    )
```

profile of v0, /device:TPU:0, one launch (start us, length us, event | category | flops | bytes accessed | tf_op | source)
XLA Modules:
  0.0 60.3 jit_solution(12747121747299165515)
XLA Ops:
  0.0 58.5 %layer.1 = bf16[256,768]{1,0:T(8,128)(2,1)} custom-call(bf16[256,3072]{1,0:T(8,128)(2,1)} %stream_hbm.1, bf16[24,128]{1,0:T(8,128)(2,1)} %bitcast.8, s32[8,256]{1,0:T(8,128)} %chosen_ref.1, f32[1,256]{1,0:T(1,128)} %aff_ref.1, bf16[3072,768]{1,0:T(8,128)(2,1)} %bitcast.5, bf16[3072,768]{1,0:T(8,128)(2,1)} %bitcast.6, bf16[768,3072]{1,0:T(8,128)(2,1)} %bitcast.7, ...), custom_call_target="tpu_custom_call" | custom-call | tf_op jit(solution)/shard_map/layer/pallas_call | solution.py:393
  58.5 1.8 %copy.10 = bf16[256,768]{1,0:T(8,128)(2,1)} copy(bf16[256,768]{1,0:T(8,128)(2,1)} %layer.1) | data formatting | bytes 786432
where the time goes:
time: 60.5 us; the launch traced here: 60.3 us
  Pallas kernels  58.5 us (97%)
  local copies, waits for them, and re-layouts  1.77 us (3%)
    pallas_call x1, Pallas kernels, on_device(): pl.pallas_call(functools.partial(layer, experts, tp, chunks, slots), out_...  58.5 us
    unnamed x1, local copies, waits for them, and re-layouts  1.77 us

commit v1 on v0

v1 whole, which is shorter than its diff:
```python
import functools

import jax
import jax.numpy as jnp
from jax import lax
from jax.experimental import pallas as pl
from jax.experimental.pallas import tpu as pltpu
from jax.sharding import PartitionSpec as P

EPSILON = 1e-06
F32 = jnp.float32
BF16 = jnp.bfloat16
I32 = jnp.int32
MESH = pl.DeviceIdType.MESH


def layer(
    experts, tp, groups, fold, slots,
    stream_hbm, gain_hbm, chosen_hbm, aff_hbm, wg_hbm, wu_hbm, wd_hbm, fgain_hbm,
    out_ref,
    x_v, xn_v, gain_v, gainf_v, chosen_v, aff_v, fgain_v, wg_v, wu_v, wd_v,
    sel_v, place_v, pack_v, spread_v, affc_v,
    send_v, recv_v, piece_v, accg_v, accu_v, hidden_v,
    psend_v, pown_v, prec_v, ysend_v, yrec_v, leave_v, ret_v, merged_v, ssq_v,
    x_sem, s_sem, wg_sem, wu_sem, wd_sem,
    dsend, drecv, gsend, grecv, fsend, frecv, psend, precv, ysend, yrecv,
    rsend, rrecv, qsend, qrecv,
):
    me = lax.axis_index("ep")
    col = lax.axis_index("tp")
    tok, width = x_v.shape
    share = width // tp
    fw = share // fold
    caps = chosen_v.shape[1]
    cg = caps // groups
    sg = slots // groups
    mr = sg * fold
    rows = experts * mr
    chips = tp // 2
    y = col // 2
    core = col % 2
    partner = y * 2 + 1 - core

    barrier = pltpu.get_barrier_semaphore()
    for r in range(1, experts):
        pl.semaphore_signal(barrier, inc=1, device_id={"ep": (me + r) % experts}, device_id_type=MESH)
    for r in range(1, tp):
        pl.semaphore_signal(barrier, inc=1, device_id={"tp": (col + r) % tp}, device_id_type=MESH)

    small = []
    for n, (src, dst) in enumerate(
        ((chosen_hbm, chosen_v), (gain_hbm, gain_v), (aff_hbm, aff_v), (fgain_hbm, fgain_v))
    ):
        copy = pltpu.make_async_copy(src, dst, s_sem.at[n])
        copy.start()
        small.append(copy)
    pieces = x_sem.shape[0]
    xrows = tok // pieces
    x_copies = []
    for i in range(pieces):
        at = pl.ds(i * xrows, xrows)
        copy = pltpu.make_async_copy(stream_hbm.at[at, :], x_v.at[at, :], x_sem.at[i])
        copy.start()
        x_copies.append(copy)

    small[0].wait()
    base = (me * tok).astype(F32)
    lane_cap = lax.broadcasted_iota(I32, (mr, caps), 1)
    lane_tok = lax.broadcasted_iota(I32, (mr, tok), 1).astype(F32)
    sub = lax.broadcasted_iota(I32, (mr, 1), 0)
    sub_half = sum((jnp.where(sub >= h * sg, 1, 0) for h in range(1, fold)), jnp.zeros((mr, 1), I32))
    sub_slot = sub - sg * sub_half

    def build_sel(e, carry):
        row = chosen_v[pl.ds(e, 1), :].astype(F32)
        start = jnp.sum(jnp.where(row < base, 1.0, 0.0), axis=1, keepdims=True).astype(I32)
        for g in range(groups):
            first = start + ((g - start) & (groups - 1))
            hit = lane_cap == first + groups * sub_slot
            token = jnp.sum(jnp.where(hit, row + 1.0, 0.0), axis=1, keepdims=True) - 1.0 - base
            for h in range(fold):
                one = (token == lane_tok) & (sub_half == h)
                sel_v[g, e, :, h * tok:(h + 1) * tok] = jnp.where(one, 1.0, 0.0).astype(BF16)
        return carry

    lax.fori_loop(0, experts, build_sel, 0, unroll=experts <= 8)

    small[1].wait()
    gainf_v[...] = gain_v[...].astype(F32)
    lines = share // 128
    gain = jnp.concatenate(
        [gainf_v[pl.ds(col * lines + i, 1), :] for i in range(lines)], axis=1
    )
    step = 32
    for i in range(pieces):
        x_copies[i].wait()
        if i == pieces - 1:
            w_copies = {}
            for r in range(chips):
                for c in range(2):
                    s = r * 2 + c
                    other = core if c == 0 else 1 - core
                    frm = ((y + chips - r) % chips) * 2 + other
                    for n, (src, dst, sem) in enumerate(((wg_hbm, wg_v, wg_sem), (wu_hbm, wu_v, wu_sem))):
                        copy = pltpu.make_async_copy(
                            src.at[pl.ds(frm * share, share), :],
                            dst.at[pl.ds(s * share, share), :],
                            sem.at[s],
                        )
                        copy.start()
                        w_copies[n, s] = copy
            for r in list(range(1, chips)) + [0]:
                for c in (1, 0):
                    s = r * 2 + c
                    other = core if c == 0 else 1 - core
                    to = ((y + r) % chips) * 2 + other
                    copy = pltpu.make_async_copy(
                        wd_hbm.at[:, pl.ds(pl.multiple_of(to * share, 128), share)],
                        wd_v.at[s], wd_sem.at[s],
                    )
                    copy.start()
                    w_copies[2, s] = copy
        for b in range(xrows // step):
            at = pl.ds(i * xrows + b * step, step)
            block = x_v[at, :].astype(F32)
            scale = lax.rsqrt(jnp.sum(block * block, axis=1, keepdims=True) / width + EPSILON)
            own = x_v[at, pl.ds(pl.multiple_of(col * share, 128), share)].astype(F32)
            normed = (own * scale * gain).astype(BF16)
            for h in range(fold):
                xn_v[pl.ds(h * tok + i * xrows + b * step, step), :] = normed[:, h * fw:(h + 1) * fw]

    finish = []
    far_first = sorted(range(1, experts), key=lambda r: -min(r, experts - r))

    def exchange(g, src, dst, ssem, rsem):
        for r in far_first:
            to = (me + r) % experts
            copy = pltpu.make_async_remote_copy(
                src_ref=src.at[g, to], dst_ref=dst.at[g, me],
                send_sem=ssem.at[g], recv_sem=rsem.at[g],
                device_id={"ep": to}, device_id_type=MESH,
            )
            copy.start()
        dst[g, me] = src[g, me]
        finish.append(whole_exchange(g, src, dst, ssem, rsem))

    def whole_exchange(g, src, dst, ssem, rsem):
        others = pl.ds(0, experts - 1)
        return pltpu.make_async_remote_copy(
            src_ref=src.at[g, others], dst_ref=dst.at[g, others],
            send_sem=ssem.at[g], recv_sem=rsem.at[g],
            device_id={"ep": (me + 1) % experts}, device_id_type=MESH,
        )

    def exchange_wait(g, src, dst, ssem, rsem):
        whole_exchange(g, src, dst, ssem, rsem).wait_recv()

    for g in range(groups):
        out = jnp.dot(sel_v[g].reshape(rows, fold * tok), xn_v[...], preferred_element_type=F32)
        send_v[g] = out.astype(BF16).reshape(experts, mr, fw)
        if g == 0:
            pl.semaphore_wait(barrier, experts - 1 + tp - 1)
        exchange(g, send_v, recv_v, dsend, drecv)

    own_row = chosen_v[pl.ds(me, 1), :].astype(F32)

    def positions(axis):
        shape = (rows, 1) if axis == 0 else (1, rows)
        j = lax.broadcasted_iota(I32, shape, axis)
        start = jnp.zeros(shape, F32)
        end = jnp.zeros(shape, F32)
        within = j
        cut = jnp.zeros((1, 1), F32)
        for d in range(experts):
            mine = (j >= d * mr) & (j < (d + 1) * mr)
            after = jnp.sum(jnp.where(own_row < float((d + 1) * tok), 1.0, 0.0), axis=1, keepdims=True)
            start = start + jnp.where(mine, cut, 0.0)
            end = end + jnp.where(mine, after, 0.0)
            within = within - jnp.where(mine, d * mr, 0)
            cut = after
        half = sum((jnp.where(within >= h * sg, 1, 0) for h in range(1, fold)), jnp.zeros(shape, I32))
        return start.astype(I32), end.astype(I32), half, within - sg * half

    for axis, dst in ((1, pack_v), (0, spread_v)):
        start, end, half, slot = positions(axis)
        for g in range(groups):
            want = start + ((g - start) & (groups - 1)) + groups * slot
            want = jnp.where(want < end, want, -1)
            for h in range(fold):
                aim = jnp.where(half == h, want, -1)
                if axis == 1:
                    pick = lax.broadcasted_iota(I32, (cg, rows), 0) * groups + g
                    pack_v[g, h * cg:(h + 1) * cg, :] = jnp.where(pick == aim, 1.0, 0.0).astype(BF16)
                else:
                    pick = lax.broadcasted_iota(I32, (rows, cg), 1) * groups + g
                    spread_v[g, :, h * cg:(h + 1) * cg] = jnp.where(pick == aim, 1.0, 0.0).astype(BF16)

    small[2].wait()
    for g in range(groups):
        lane = lax.broadcasted_iota(I32, (cg, caps), 1)
        pick = lax.broadcasted_iota(I32, (cg, caps), 0) * groups + g
        affc_v[g] = jnp.sum(jnp.where(lane == pick, aff_v[...], 0.0), axis=1, keepdims=True)

    for g in range(groups):
        whole = sel_v[g].reshape(rows, fold * tok).astype(F32)
        place_v[g] = whole.T.astype(BF16)

    def gather_start(g):
        exchange_wait(g, send_v, recv_v, dsend, drecv)
        got = recv_v[g].reshape(rows, fw)
        piece_v[g, 0] = jnp.dot(pack_v[g], got, preferred_element_type=F32).astype(BF16)
        for r in range(1, chips):
            to = ((y + r) % chips) * 2 + core
            copy = pltpu.make_async_remote_copy(
                src_ref=piece_v.at[g, 0], dst_ref=piece_v.at[g, 2 * r],
                send_sem=gsend.at[g, r], recv_sem=grecv.at[g, r],
                device_id={"tp": to}, device_id_type=MESH,
            )
            copy.start()
            finish.append(copy)
        forward(g, 0)

    def forward_copy(g, r):
        return pltpu.make_async_remote_copy(
            src_ref=piece_v.at[g, 2 * r], dst_ref=piece_v.at[g, 2 * r + 1],
            send_sem=fsend.at[g, r], recv_sem=frecv.at[g, r],
            device_id={"tp": partner}, device_id_type=MESH,
        )

    def forward(g, r):
        copy = forward_copy(g, r)
        copy.start()
        finish.append(copy)

    def gather_forward(g):
        for r in range(1, chips):
            frm = ((y + chips - r) % chips) * 2 + core
            pltpu.make_async_remote_copy(
                src_ref=piece_v.at[g, 0], dst_ref=piece_v.at[g, 2 * r],
                send_sem=gsend.at[g, r], recv_sem=grecv.at[g, r],
                device_id={"tp": frm}, device_id_type=MESH,
            ).wait_recv()
            forward(g, r)

    waited = set()

    def weight_wait(n, s):
        if (n, s) not in waited:
            waited.add((n, s))
            w_copies[n, s].wait()

    def contract(g, lo, hi):
        taken = jnp.concatenate(
            [piece_v[g, s, h * cg:(h + 1) * cg, :] for s in range(lo, hi) for h in range(fold)], axis=1
        )
        for n in range(2):
            for s in range(lo, hi):
                weight_wait(n, s)
        at = pl.ds(lo * share, (hi - lo) * share)
        gate = jnp.dot(taken, wg_v[at, :], preferred_element_type=F32)
        up = jnp.dot(taken, wu_v[at, :], preferred_element_type=F32)
        return gate, up

    def near(g):
        forward_copy(g, 0).wait_recv()
        gate, up = contract(g, 0, 2)
        accg_v[g] = gate
        accu_v[g] = up

    def pair_copy(g, r):
        return pltpu.make_async_remote_copy(
            src_ref=psend_v.at[g, r], dst_ref=prec_v.at[g, r],
            send_sem=psend.at[g, r], recv_sem=precv.at[g, r],
            device_id={"tp": partner}, device_id_type=MESH,
        )

    def far(g):
        for r in range(1, chips):
            forward_copy(g, r).wait_recv()
        gate, up = contract(g, 2, tp)
        gate = gate + accg_v[g]
        up = up + accu_v[g]
        hidden_v[g] = (gate / (1.0 + jnp.exp(-gate)) * up).astype(BF16)
        for turns in (list(range(1, chips)), [0]):
            for r in turns:
                weight_wait(2, 2 * r + 1)
                psend_v[g, r] = jnp.dot(hidden_v[g], wd_v[2 * r + 1], preferred_element_type=F32).astype(BF16)
                copy = pair_copy(g, r)
                copy.start()
                finish.append(copy)
            for r in turns:
                weight_wait(2, 2 * r)
                pown_v[g, r] = jnp.dot(hidden_v[g], wd_v[2 * r], preferred_element_type=F32)

    def chip_copy(g, r):
        to = ((y + r) % chips) * 2 + core
        return pltpu.make_async_remote_copy(
            src_ref=ysend_v.at[g, r], dst_ref=yrec_v.at[g, r],
            send_sem=ysend.at[g, r], recv_sem=yrecv.at[g, r],
            device_id={"tp": to}, device_id_type=MESH,
        )

    def cross(g):
        for r in range(1, chips):
            pair_copy(g, r).wait_recv()
            ysend_v[g, r] = (pown_v[g, r] + prec_v[g, r].astype(F32)).astype(BF16)
            copy = chip_copy(g, r)
            copy.start()
            finish.append(copy)

    def leave(g):
        pair_copy(g, 0).wait_recv()
        total = pown_v[g, 0] + prec_v[g, 0].astype(F32)
        for r in range(1, chips):
            chip_copy(g, r).wait_recv()
            total = total + yrec_v[g, r].astype(F32)
        weighted = (total * affc_v[g]).astype(BF16)
        folded = jnp.concatenate([weighted[:, h * fw:(h + 1) * fw] for h in range(fold)], axis=0)
        out = jnp.dot(spread_v[g], folded, preferred_element_type=F32)
        leave_v[g] = out.astype(BF16).reshape(experts, mr, fw)
        exchange(g, leave_v, ret_v, rsend, rrecv)

    def settle(g):
        exchange_wait(g, leave_v, ret_v, rsend, rrecv)
        update = jnp.dot(place_v[g], ret_v[g].reshape(rows, fw), preferred_element_type=F32)
        if g == 0:
            for h in range(fold):
                at = pl.ds(pl.multiple_of(col * share + h * fw, 128), fw)
                merged_v[h * tok:(h + 1) * tok, :] = x_v[:, at].astype(F32) + update[h * tok:(h + 1) * tok, :]
        else:
            merged_v[...] = merged_v[...] + update

    stages = {
        "s1": gather_start, "s2": gather_forward, "a": near, "b": far, "x": cross, "l": leave, "r": settle,
    }
    if groups == 4:
        order = ORDER4
    else:
        order = [f"{name}.{g}" for name in ("s1", "s2", "a", "b", "x", "l", "r") for g in range(groups)]
    for item in order:
        name, g = item.split(".")
        with jax.named_scope(name + g):
            stages[name](int(g))

    square = 128
    eye = (
        lax.broadcasted_iota(I32, (square, square), 0)
        == lax.broadcasted_iota(I32, (square, square), 1)
    )
    merged = merged_v[...]
    both = jnp.sum(merged * merged, axis=1, keepdims=True)
    squares = both[0:tok]
    for h in range(1, fold):
        squares = squares + both[h * tok:(h + 1) * tok]
    for b in range(tok // square):
        line = jnp.sum(
            jnp.where(eye, squares[b * square:(b + 1) * square, :], 0.0), axis=0, keepdims=True
        )
        ssq_v[0, :, b * square:(b + 1) * square] = jnp.broadcast_to(line, (8, square))

    def square_copy(r):
        return pltpu.make_async_remote_copy(
            src_ref=ssq_v.at[0], dst_ref=ssq_v.at[r],
            send_sem=qsend.at[r], recv_sem=qrecv.at[r],
            device_id={"tp": (col + r) % tp}, device_id_type=MESH,
        )

    for r in range(1, tp):
        copy = square_copy(r)
        copy.start()
        finish.append(copy)
    small[3].wait()
    closing = fgain_v[...].astype(F32)
    fgain = jnp.concatenate([closing[i:i + 1, :] for i in range(lines)], axis=1)
    sums = ssq_v[0]
    with jax.named_scope("sqw"):
        for r in range(1, tp):
            square_copy(r).wait_recv()
            sums = sums + ssq_v[r]
    scales = lax.rsqrt(sums[0:1, :] / width + EPSILON)
    for b in range(tok // square):
        line = scales[:, b * square:(b + 1) * square]
        column = jnp.sum(jnp.where(eye, line, 0.0), axis=1, keepdims=True)
        for h in range(fold):
            part = merged_v[h * tok + b * square:h * tok + (b + 1) * square, :]
            out_ref[b * square:(b + 1) * square, h * fw:(h + 1) * fw] = (
                part * column * fgain[:, h * fw:(h + 1) * fw]
            ).astype(BF16)

    with jax.named_scope("fin"):
        for copy in finish:
            copy.wait_send()


ORDER4 = [
    "s1.0", "a.0", "s1.1", "s2.0", "b.0", "s1.2", "a.1", "s2.1", "x.0", "a.2", "b.1",
    "s1.3", "s2.2", "x.1", "l.0", "b.2", "a.3", "s2.3", "x.2", "l.1", "b.3", "x.3", "l.2",
    "r.0", "l.3", "r.1", "r.2", "r.3",
]


def on_device(stream, ffn_gain, chosen, affinity, w_gate, w_up, w_down, final_gain):
    tok, width = stream.shape
    experts, caps = chosen.shape
    tp = lax.axis_size("tp")
    share = width // tp
    hid = w_gate.shape[2]
    slots = 3 * tok // 16
    groups, fold = (4, 2) if share % 256 == 0 else (2, 1)
    fw = share // fold
    cg = caps // groups
    mr = slots // groups * fold
    rows = experts * mr
    chips = tp // 2
    hbm = pl.BlockSpec(memory_space=pltpu.HBM)
    dma = pltpu.SemaphoreType.DMA
    buffers = [
        pltpu.VMEM((tok, width), BF16),
        pltpu.VMEM((fold * tok, fw), BF16),
        pltpu.VMEM((width // 128, 128), BF16),
        pltpu.VMEM((width // 128, 128), F32),
        pltpu.VMEM((experts, caps), I32),
        pltpu.VMEM((1, caps), F32),
        pltpu.VMEM((share // 128, 128), BF16),
        pltpu.VMEM((width, hid), BF16),
        pltpu.VMEM((width, hid), BF16),
        pltpu.VMEM((tp, hid, share), BF16),
        pltpu.VMEM((groups, experts, mr, fold * tok), BF16),
        pltpu.VMEM((groups, fold * tok, rows), BF16),
        pltpu.VMEM((groups, fold * cg, rows), BF16),
        pltpu.VMEM((groups, rows, fold * cg), BF16),
        pltpu.VMEM((groups, cg, 1), F32),
        pltpu.VMEM((groups, experts, mr, fw), BF16),
        pltpu.VMEM((groups, experts, mr, fw), BF16),
        pltpu.VMEM((groups, tp, fold * cg, fw), BF16),
        pltpu.VMEM((groups, cg, hid), F32),
        pltpu.VMEM((groups, cg, hid), F32),
        pltpu.VMEM((groups, cg, hid), BF16),
        pltpu.VMEM((groups, chips, cg, share), BF16),
        pltpu.VMEM((groups, chips, cg, share), F32),
        pltpu.VMEM((groups, chips, cg, share), BF16),
        pltpu.VMEM((groups, chips, cg, share), BF16),
        pltpu.VMEM((groups, chips, cg, share), BF16),
        pltpu.VMEM((groups, experts, mr, fw), BF16),
        pltpu.VMEM((groups, experts, mr, fw), BF16),
        pltpu.VMEM((fold * tok, fw), F32),
        pltpu.VMEM((tp, 8, tok), F32),
    ]
    return pl.pallas_call(
        functools.partial(layer, experts, tp, groups, fold, slots),
        out_shape=pltpu.VMEM((tok, share), BF16),
        in_specs=[hbm] * 8,
        out_specs=pl.BlockSpec(memory_space=pltpu.VMEM),
        scratch_shapes=buffers + [
            dma((4,)), dma((4,)), dma((tp,)), dma((tp,)), dma((tp,)),
            dma((groups,)), dma((groups,)),
            dma((groups, chips)), dma((groups, chips)),
            dma((groups, chips)), dma((groups, chips)),
            dma((groups, chips)), dma((groups, chips)),
            dma((groups, chips)), dma((groups, chips)),
            dma((groups,)), dma((groups,)),
            dma((tp,)), dma((tp,)),
        ],
        compiler_params=pltpu.CompilerParams(
            collective_id=0, has_side_effects=True, vmem_limit_bytes=56 * 1024 * 1024
        ),
        name="layer",
    )(
        stream,
        ffn_gain.reshape(width // 128, 128),
        chosen,
        affinity,
        w_gate[0],
        w_up[0],
        w_down[0],
        final_gain.reshape(share // 128, 128),
    )


def solution(mesh):
    return jax.shard_map(
        on_device,
        mesh=mesh,
        in_specs=(
            P("ep", None),
            P(),
            P(),
            P("ep", None),
            P("ep", None, "tp"),
            P("ep", None, "tp"),
            P("ep", "tp", None),
            P("tp"),
        ),
        out_specs=P("ep", "tp"),
        check_vma=False,
    )
```

time: 60.5 us -> 49.8 us (0.82)
  Pallas kernels: 58.5 us -> 48.8 us
  local copies, waits for them, and re-layouts: 1.77 us -> 0.75 us
    pallas_call x1, Pallas kernels: 58.5 us -> 48.8 us  [on_device(): pl.pallas_call(functools.partial(layer, experts, tp, groups, fold, slots)...]
    unnamed x1, local copies, waits for them, and re-layouts: 1.77 us -> 0.75 us
where the time goes in v1:
time: 49.8 us; the launch traced here: 49.6 us
  Pallas kernels  48.8 us (98%)
  local copies, waits for them, and re-layouts  0.75 us (2%)
    pallas_call x1, Pallas kernels, on_device(): pl.pallas_call(functools.partial(layer, experts, tp, groups, fold, slots)...  48.8 us

profile of v1, /device:TPU:0, one launch (start us, length us, event | category | flops | bytes accessed | tf_op | source)
XLA Modules:
  0.0 49.6 jit_solution(2213001522350012406)
XLA Ops:
  0.0 48.8 %layer.1 = bf16[256,768]{1,0:T(8,128)(2,1)S(1)} custom-call(bf16[256,3072]{1,0:T(8,128)(2,1)} %stream_hbm.1, bf16[24,128]{1,0:T(8,128)(2,1)} %bitcast.8, s32[8,256]{1,0:T(8,128)} %chosen_hbm.1, f32[1,256]{1,0:T(1,128)} %aff_hbm.1, bf16[3072,768]{1,0:T(8,128)(2,1)} %bitcast.5, bf16[3072,768]{1,0:T(8,128)(2,1)} %bitcast.6, bf16[768,3072]{1,0:T(8,128)(2,1)} %bitcast.7, ...), custom_call_target="tpu_custom_call" | custom-call | tf_op jit(solution)/shard_map/layer/pallas_call | solution.py:449
  48.8 0.7 %copy.10 = bf16[256,768]{1,0:T(8,128)(2,1)} copy(bf16[256,768]{1,0:T(8,128)(2,1)S(1)} %layer.1) | data formatting | bytes 786432

commit v2 on v1

--- a/solution.py
+++ b/solution.py
@@ -43,9 +43,17 @@
 
     barrier = pltpu.get_barrier_semaphore()
     for r in range(1, experts):
-        pl.semaphore_signal(barrier, inc=1, device_id={"ep": (me + r) % experts}, device_id_type=MESH)
+        pl.semaphore_signal(barrier, inc=1, device_id={"ep": (me + r) % experts, "tp": partner}, device_id_type=MESH)
     for r in range(1, tp):
         pl.semaphore_signal(barrier, inc=1, device_id={"tp": (col + r) % tp}, device_id_type=MESH)
+
+    gather_cols = [col, partner]
+    scatter_cols = [partner, col]
+    for r in range(1, chips):
+        before = (y + chips - r) % chips * 2
+        after = (y + r) % chips * 2
+        gather_cols += [before + 1 - core, before + core]
+        scatter_cols += [after + core, after + 1 - core]
 
     small = []
     for n, (src, dst) in enumerate(
@@ -89,71 +97,46 @@
     gainf_v[...] = gain_v[...].astype(F32)
     lines = share // 128
     gain = jnp.concatenate(
-        [gainf_v[pl.ds(col * lines + i, 1), :] for i in range(lines)], axis=1
+        [gainf_v[pl.ds(partner * lines + i, 1), :] for i in range(lines)], axis=1
     )
     step = 32
     for i in range(pieces):
         x_copies[i].wait()
         if i == pieces - 1:
-            w_copies = {}
-            for r in range(chips):
-                for c in range(2):
-                    s = r * 2 + c
-                    other = core if c == 0 else 1 - core
-                    frm = ((y + chips - r) % chips) * 2 + other
-                    for n, (src, dst, sem) in enumerate(((wg_hbm, wg_v, wg_sem), (wu_hbm, wu_v, wu_sem))):
-                        copy = pltpu.make_async_copy(
-                            src.at[pl.ds(frm * share, share), :],
-                            dst.at[pl.ds(s * share, share), :],
-                            sem.at[s],
-                        )
-                        copy.start()
-                        w_copies[n, s] = copy
-            for r in list(range(1, chips)) + [0]:
-                for c in (1, 0):
-                    s = r * 2 + c
-                    other = core if c == 0 else 1 - core
-                    to = ((y + r) % chips) * 2 + other
-                    copy = pltpu.make_async_copy(
-                        wd_hbm.at[:, pl.ds(pl.multiple_of(to * share, 128), share)],
-                        wd_v.at[s], wd_sem.at[s],
-                    )
-                    copy.start()
-                    w_copies[2, s] = copy
+            for s, frm in enumerate(gather_cols):
+                for src, dst, sem in ((wg_hbm, wg_v, wg_sem), (wu_hbm, wu_v, wu_sem)):
+                    pltpu.make_async_copy(
+                        src.at[pl.ds(frm * share, share), :],
+                        dst.at[pl.ds(s * share, share), :],
+                        sem.at[0 if s < 2 else 1 + s % 2],
+                    ).start()
+            for s, to in enumerate(scatter_cols):
+                pltpu.make_async_copy(
+                    wd_hbm.at[:, pl.ds(pl.multiple_of(to * share, 128), share)],
+                    wd_v.at[s], wd_sem,
+                ).start()
         for b in range(xrows // step):
             at = pl.ds(i * xrows + b * step, step)
             block = x_v[at, :].astype(F32)
             scale = lax.rsqrt(jnp.sum(block * block, axis=1, keepdims=True) / width + EPSILON)
-            own = x_v[at, pl.ds(pl.multiple_of(col * share, 128), share)].astype(F32)
+            own = x_v[at, pl.ds(pl.multiple_of(partner * share, 128), share)].astype(F32)
             normed = (own * scale * gain).astype(BF16)
             for h in range(fold):
                 xn_v[pl.ds(h * tok + i * xrows + b * step, step), :] = normed[:, h * fw:(h + 1) * fw]
 
-    finish = []
-    far_first = sorted(range(1, experts), key=lambda r: -min(r, experts - r))
+    far_first = sorted(range(experts), key=lambda r: -min(r, experts - r))
 
     def exchange(g, src, dst, ssem, rsem):
         for r in far_first:
             to = (me + r) % experts
-            copy = pltpu.make_async_remote_copy(
+            pltpu.make_async_remote_copy(
                 src_ref=src.at[g, to], dst_ref=dst.at[g, me],
-                send_sem=ssem.at[g], recv_sem=rsem.at[g],
-                device_id={"ep": to}, device_id_type=MESH,
-            )
-            copy.start()
-        dst[g, me] = src[g, me]
-        finish.append(whole_exchange(g, src, dst, ssem, rsem))
-
-    def whole_exchange(g, src, dst, ssem, rsem):
-        others = pl.ds(0, experts - 1)
-        return pltpu.make_async_remote_copy(
-            src_ref=src.at[g, others], dst_ref=dst.at[g, others],
-            send_sem=ssem.at[g], recv_sem=rsem.at[g],
-            device_id={"ep": (me + 1) % experts}, device_id_type=MESH,
-        )
-
-    def exchange_wait(g, src, dst, ssem, rsem):
-        whole_exchange(g, src, dst, ssem, rsem).wait_recv()
+                send_sem=ssem, recv_sem=rsem.at[g],
+                device_id={"ep": to, "tp": partner}, device_id_type=MESH,
+            ).start()
+
+    def remote_wait(ref, sem):
+        pltpu.make_async_copy(ref, ref, sem).wait()
 
     for g in range(groups):
         out = jnp.dot(sel_v[g].reshape(rows, fold * tok), xn_v[...], preferred_element_type=F32)
@@ -206,113 +189,114 @@
         place_v[g] = whole.T.astype(BF16)
 
     def gather_start(g):
-        exchange_wait(g, send_v, recv_v, dsend, drecv)
+        remote_wait(recv_v.at[g], drecv.at[g])
         got = recv_v[g].reshape(rows, fw)
         piece_v[g, 0] = jnp.dot(pack_v[g], got, preferred_element_type=F32).astype(BF16)
         for r in range(1, chips):
-            to = ((y + r) % chips) * 2 + core
-            copy = pltpu.make_async_remote_copy(
-                src_ref=piece_v.at[g, 0], dst_ref=piece_v.at[g, 2 * r],
-                send_sem=gsend.at[g, r], recv_sem=grecv.at[g, r],
-                device_id={"tp": to}, device_id_type=MESH,
-            )
-            copy.start()
-            finish.append(copy)
-        forward(g, 0)
-
-    def forward_copy(g, r):
-        return pltpu.make_async_remote_copy(
-            src_ref=piece_v.at[g, 2 * r], dst_ref=piece_v.at[g, 2 * r + 1],
-            send_sem=fsend.at[g, r], recv_sem=frecv.at[g, r],
-            device_id={"tp": partner}, device_id_type=MESH,
-        )
-
-    def forward(g, r):
-        copy = forward_copy(g, r)
-        copy.start()
-        finish.append(copy)
-
-    def gather_forward(g):
-        for r in range(1, chips):
-            frm = ((y + chips - r) % chips) * 2 + core
             pltpu.make_async_remote_copy(
                 src_ref=piece_v.at[g, 0], dst_ref=piece_v.at[g, 2 * r],
-                send_sem=gsend.at[g, r], recv_sem=grecv.at[g, r],
-                device_id={"tp": frm}, device_id_type=MESH,
-            ).wait_recv()
+                send_sem=gsend, recv_sem=grecv.at[g],
+                device_id={"tp": (y + r) % chips * 2 + 1 - core}, device_id_type=MESH,
+            ).start()
+        forward(g, 0)
+
+    def forward(g, r):
+        pltpu.make_async_remote_copy(
+            src_ref=piece_v.at[g, 2 * r], dst_ref=piece_v.at[g, 2 * r + 1],
+            send_sem=fsend, recv_sem=frecv.at[g, min(r, 1)],
+            device_id={"tp": partner}, device_id_type=MESH,
+        ).start()
+
+    def gather_forward(g):
+        remote_wait(piece_v.at[g, pl.ds(0, chips - 1)], grecv.at[g])
+        for r in range(1, chips):
             forward(g, r)
 
     waited = set()
 
-    def weight_wait(n, s):
-        if (n, s) not in waited:
-            waited.add((n, s))
-            w_copies[n, s].wait()
-
-    def contract(g, lo, hi):
+    def weight_wait(n):
+        if n not in waited:
+            waited.add(n)
+            if n == 3:
+                remote_wait(wd_v, wd_sem)
+            else:
+                at = pl.ds(0, (2 if n == 0 else chips - 1) * share)
+                remote_wait(wg_v.at[at, :], wg_sem.at[n])
+                remote_wait(wu_v.at[at, :], wu_sem.at[n])
+
+    def contract(g, slots_in):
         taken = jnp.concatenate(
-            [piece_v[g, s, h * cg:(h + 1) * cg, :] for s in range(lo, hi) for h in range(fold)], axis=1
+            [piece_v[g, s, h * cg:(h + 1) * cg, :] for s in slots_in for h in range(fold)], axis=1
         )
-        for n in range(2):
-            for s in range(lo, hi):
-                weight_wait(n, s)
-        at = pl.ds(lo * share, (hi - lo) * share)
-        gate = jnp.dot(taken, wg_v[at, :], preferred_element_type=F32)
-        up = jnp.dot(taken, wu_v[at, :], preferred_element_type=F32)
-        return gate, up
+        if slots_in == [0, 1]:
+            return [
+                jnp.dot(taken, w[0:2 * share, :], preferred_element_type=F32) for w in (wg_v, wu_v)
+            ]
+        return [
+            sum(
+                jnp.dot(
+                    taken[:, n * share:(n + 1) * share], w[s * share:(s + 1) * share, :],
+                    preferred_element_type=F32,
+                )
+                for n, s in enumerate(slots_in)
+            )
+            for w in (wg_v, wu_v)
+        ]
 
     def near(g):
-        forward_copy(g, 0).wait_recv()
-        gate, up = contract(g, 0, 2)
-        accg_v[g] = gate
-        accu_v[g] = up
-
-    def pair_copy(g, r):
-        return pltpu.make_async_remote_copy(
-            src_ref=psend_v.at[g, r], dst_ref=prec_v.at[g, r],
-            send_sem=psend.at[g, r], recv_sem=precv.at[g, r],
-            device_id={"tp": partner}, device_id_type=MESH,
-        )
-
-    def far(g):
-        for r in range(1, chips):
-            forward_copy(g, r).wait_recv()
-        gate, up = contract(g, 2, tp)
+        remote_wait(piece_v.at[g, 1], frecv.at[g, 0])
+        weight_wait(0)
+        accg_v[g], accu_v[g] = contract(g, [0, 1])
+
+    def middle(g):
+        weight_wait(1)
+        gate, up = contract(g, [2 * r for r in range(1, chips)])
+        accg_v[g] += gate
+        accu_v[g] += up
+
+    def away(g):
+        remote_wait(piece_v.at[g, pl.ds(0, chips - 1)], frecv.at[g, 1])
+        weight_wait(2)
+        gate, up = contract(g, [2 * r + 1 for r in range(1, chips)])
         gate = gate + accg_v[g]
         up = up + accu_v[g]
         hidden_v[g] = (gate / (1.0 + jnp.exp(-gate)) * up).astype(BF16)
-        for turns in (list(range(1, chips)), [0]):
-            for r in turns:
-                weight_wait(2, 2 * r + 1)
-                psend_v[g, r] = jnp.dot(hidden_v[g], wd_v[2 * r + 1], preferred_element_type=F32).astype(BF16)
-                copy = pair_copy(g, r)
-                copy.start()
-                finish.append(copy)
-            for r in turns:
-                weight_wait(2, 2 * r)
-                pown_v[g, r] = jnp.dot(hidden_v[g], wd_v[2 * r], preferred_element_type=F32)
-
-    def chip_copy(g, r):
-        to = ((y + r) % chips) * 2 + core
-        return pltpu.make_async_remote_copy(
-            src_ref=ysend_v.at[g, r], dst_ref=yrec_v.at[g, r],
-            send_sem=ysend.at[g, r], recv_sem=yrecv.at[g, r],
-            device_id={"tp": to}, device_id_type=MESH,
-        )
+        weight_wait(3)
+        for r in range(1, chips):
+            pair(g, r)
+
+    def down(g, s):
+        return jnp.dot(hidden_v[g], wd_v[s], preferred_element_type=F32)
+
+    def pair(g, r):
+        psend_v[g, r] = down(g, 2 * r + 1).astype(BF16)
+        pltpu.make_async_remote_copy(
+            src_ref=psend_v.at[g, r], dst_ref=prec_v.at[g, r],
+            send_sem=psend, recv_sem=precv.at[g, min(r, 1)],
+            device_id={"tp": partner}, device_id_type=MESH,
+        ).start()
+
+    def home(g):
+        for r in range(1, chips):
+            pown_v[g, r] = down(g, 2 * r)
+        pair(g, 0)
 
     def cross(g):
-        for r in range(1, chips):
-            pair_copy(g, r).wait_recv()
+        remote_wait(prec_v.at[g, pl.ds(0, chips - 1)], precv.at[g, 1])
+        for r in range(1, chips):
             ysend_v[g, r] = (pown_v[g, r] + prec_v[g, r].astype(F32)).astype(BF16)
-            copy = chip_copy(g, r)
-            copy.start()
-            finish.append(copy)
+            pltpu.make_async_remote_copy(
+                src_ref=ysend_v.at[g, r], dst_ref=yrec_v.at[g, r],
+                send_sem=ysend, recv_sem=yrecv.at[g],
+                device_id={"tp": (y + r) % chips * 2 + 1 - core}, device_id_type=MESH,
+            ).start()
+        pown_v[g, 0] = down(g, 0)
 
     def leave(g):
-        pair_copy(g, 0).wait_recv()
+        remote_wait(prec_v.at[g, 0], precv.at[g, 0])
         total = pown_v[g, 0] + prec_v[g, 0].astype(F32)
-        for r in range(1, chips):
-            chip_copy(g, r).wait_recv()
+        remote_wait(yrec_v.at[g, pl.ds(0, chips - 1)], yrecv.at[g])
+        for r in range(1, chips):
             total = total + yrec_v[g, r].astype(F32)
         weighted = (total * affc_v[g]).astype(BF16)
         folded = jnp.concatenate([weighted[:, h * fw:(h + 1) * fw] for h in range(fold)], axis=0)
@@ -321,7 +305,7 @@
         exchange(g, leave_v, ret_v, rsend, rrecv)
 
     def settle(g):
-        exchange_wait(g, leave_v, ret_v, rsend, rrecv)
+        remote_wait(ret_v.at[g], rrecv.at[g])
         update = jnp.dot(place_v[g], ret_v[g].reshape(rows, fw), preferred_element_type=F32)
         if g == 0:
             for h in range(fold):
@@ -331,12 +315,13 @@
             merged_v[...] = merged_v[...] + update
 
     stages = {
-        "s1": gather_start, "s2": gather_forward, "a": near, "b": far, "x": cross, "l": leave, "r": settle,
+        "s1": gather_start, "s2": gather_forward, "a": near, "m": middle, "b": away, "h": home,
+        "x": cross, "l": leave, "r": settle,
     }
     if groups == 4:
         order = ORDER4
     else:
-        order = [f"{name}.{g}" for name in ("s1", "s2", "a", "b", "x", "l", "r") for g in range(groups)]
+        order = [f"{name}.{g}" for name in ("s1", "s2", "a", "m", "b", "h", "x", "l", "r") for g in range(groups)]
     for item in order:
         name, g = item.split(".")
         with jax.named_scope(name + g):
@@ -361,21 +346,19 @@
     def square_copy(r):
         return pltpu.make_async_remote_copy(
             src_ref=ssq_v.at[0], dst_ref=ssq_v.at[r],
-            send_sem=qsend.at[r], recv_sem=qrecv.at[r],
+            send_sem=qsend, recv_sem=qrecv,
             device_id={"tp": (col + r) % tp}, device_id_type=MESH,
         )
 
     for r in range(1, tp):
-        copy = square_copy(r)
-        copy.start()
-        finish.append(copy)
+        square_copy(r).start()
     small[3].wait()
     closing = fgain_v[...].astype(F32)
     fgain = jnp.concatenate([closing[i:i + 1, :] for i in range(lines)], axis=1)
     sums = ssq_v[0]
     with jax.named_scope("sqw"):
+        remote_wait(ssq_v.at[pl.ds(1, tp - 1)], qrecv)
         for r in range(1, tp):
-            square_copy(r).wait_recv()
             sums = sums + ssq_v[r]
     scales = lax.rsqrt(sums[0:1, :] / width + EPSILON)
     for b in range(tok // square):
@@ -388,14 +371,19 @@
             ).astype(BF16)
 
     with jax.named_scope("fin"):
-        for copy in finish:
-            copy.wait_send()
+        remote_wait(send_v, dsend)
+        remote_wait(piece_v.at[:, pl.ds(0, chips - 1)], gsend)
+        remote_wait(piece_v.at[:, pl.ds(0, chips)], fsend)
+        remote_wait(psend_v, psend)
+        remote_wait(ysend_v.at[:, pl.ds(0, chips - 1)], ysend)
+        remote_wait(leave_v, rsend)
+        remote_wait(ssq_v.at[pl.ds(1, tp - 1)], qsend)
 
 
 ORDER4 = [
-    "s1.0", "a.0", "s1.1", "s2.0", "b.0", "s1.2", "a.1", "s2.1", "x.0", "a.2", "b.1",
-    "s1.3", "s2.2", "x.1", "l.0", "b.2", "a.3", "s2.3", "x.2", "l.1", "b.3", "x.3", "l.2",
-    "r.0", "l.3", "r.1", "r.2", "r.3",
+    "s1.0", "a.0", "s1.1", "s2.0", "m.0", "a.1", "b.0", "h.0", "s1.2", "s2.1", "x.0", "m.1", "a.2", "b.1", "h.1",
+    "s1.3", "s2.2", "x.1", "m.2", "l.0", "b.2", "h.2", "a.3", "x.2", "s2.3", "m.3", "l.1", "b.3", "h.3",
+    "x.3", "l.2", "r.0", "l.3", "r.1", "r.2", "r.3",
 ]
 
 
@@ -452,14 +440,9 @@
         in_specs=[hbm] * 8,
         out_specs=pl.BlockSpec(memory_space=pltpu.VMEM),
         scratch_shapes=buffers + [
-            dma((4,)), dma((4,)), dma((tp,)), dma((tp,)), dma((tp,)),
-            dma((groups,)), dma((groups,)),
-            dma((groups, chips)), dma((groups, chips)),
-            dma((groups, chips)), dma((groups, chips)),
-            dma((groups, chips)), dma((groups, chips)),
-            dma((groups, chips)), dma((groups, chips)),
-            dma((groups,)), dma((groups,)),
-            dma((tp,)), dma((tp,)),
+            dma((4,)), dma((4,)), dma((3,)), dma((3,)), dma,
+            dma, dma((groups,)), dma, dma((groups,)), dma, dma((groups, 2)),
+            dma, dma((groups, 2)), dma, dma((groups,)), dma, dma((groups,)), dma, dma,
         ],
         compiler_params=pltpu.CompilerParams(
             collective_id=0, has_side_effects=True, vmem_limit_bytes=56 * 1024 * 1024

time: 49.8 us -> 46.3 us (0.930)
  Pallas kernels: 48.8 us -> 45.3 us
    pallas_call x1, Pallas kernels: 48.8 us -> 45.3 us  [on_device(): pl.pallas_call(functools.partial(layer, experts, tp, groups, fold, slots)...]
where the time goes in v2:
time: 46.3 us; the launch traced here: 46.1 us
  Pallas kernels  45.3 us (98%)
  local copies, waits for them, and re-layouts  0.75 us (2%)
    pallas_call x1, Pallas kernels, on_device(): pl.pallas_call(functools.partial(layer, experts, tp, groups, fold, slots)...  45.3 us

profile of v2, /device:TPU:0, one launch (start us, length us, event | category | flops | bytes accessed | tf_op | source)
XLA Modules:
  0.0 46.1 jit_solution(17443407409939732820)
XLA Ops:
  0.0 45.3 %layer.1 = bf16[256,768]{1,0:T(8,128)(2,1)S(1)} custom-call(bf16[256,3072]{1,0:T(8,128)(2,1)} %stream_hbm.1, bf16[24,128]{1,0:T(8,128)(2,1)} %bitcast.8, s32[8,256]{1,0:T(8,128)} %chosen_hbm.1, f32[1,256]{1,0:T(1,128)} %aff_hbm.1, bf16[3072,768]{1,0:T(8,128)(2,1)} %bitcast.5, bf16[3072,768]{1,0:T(8,128)(2,1)} %bitcast.6, bf16[768,3072]{1,0:T(8,128)(2,1)} %bitcast.7, ...), custom_call_target="tpu_custom_call" | custom-call | tf_op jit(solution)/shard_map/layer/pallas_call | solution.py:437
  45.4 0.7 %copy.10 = bf16[256,768]{1,0:T(8,128)(2,1)} copy(bf16[256,768]{1,0:T(8,128)(2,1)S(1)} %layer.1) | data formatting | bytes 786432

commit v3 on v2

--- a/solution.py
+++ b/solution.py
@@ -79,20 +79,21 @@
     sub_half = sum((jnp.where(sub >= h * sg, 1, 0) for h in range(1, fold)), jnp.zeros((mr, 1), I32))
     sub_slot = sub - sg * sub_half
 
-    def build_sel(e, carry):
-        row = chosen_v[pl.ds(e, 1), :].astype(F32)
-        start = jnp.sum(jnp.where(row < base, 1.0, 0.0), axis=1, keepdims=True).astype(I32)
-        for g in range(groups):
+    def build_sel(g):
+        def one_expert(e, carry):
+            row = chosen_v[pl.ds(e, 1), :].astype(F32)
+            start = jnp.sum(jnp.where(row < base, 1.0, 0.0), axis=1, keepdims=True).astype(I32)
             first = start + ((g - start) & (groups - 1))
             hit = lane_cap == first + groups * sub_slot
             token = jnp.sum(jnp.where(hit, row + 1.0, 0.0), axis=1, keepdims=True) - 1.0 - base
             for h in range(fold):
                 one = (token == lane_tok) & (sub_half == h)
                 sel_v[g, e, :, h * tok:(h + 1) * tok] = jnp.where(one, 1.0, 0.0).astype(BF16)
-        return carry
-
-    lax.fori_loop(0, experts, build_sel, 0, unroll=experts <= 8)
-
+            return carry
+
+        lax.fori_loop(0, experts, one_expert, 0, unroll=experts <= 8)
+
+    build_sel(0)
     small[1].wait()
     gainf_v[...] = gain_v[...].astype(F32)
     lines = share // 128
@@ -125,10 +126,17 @@
                 xn_v[pl.ds(h * tok + i * xrows + b * step, step), :] = normed[:, h * fw:(h + 1) * fw]
 
     far_first = sorted(range(experts), key=lambda r: -min(r, experts - r))
+    half_n = experts // 2
+    side = me // half_n
+
+    def target(i):
+        if i < half_n:
+            return (1 - side) * half_n + (me + i) % half_n
+        return side * half_n + (me + i + 1) % half_n
 
     def exchange(g, src, dst, ssem, rsem):
-        for r in far_first:
-            to = (me + r) % experts
+        for i in range(experts):
+            to = (me + far_first[i]) % experts
             pltpu.make_async_remote_copy(
                 src_ref=src.at[g, to], dst_ref=dst.at[g, me],
                 send_sem=ssem, recv_sem=rsem.at[g],
@@ -138,12 +146,16 @@
     def remote_wait(ref, sem):
         pltpu.make_async_copy(ref, ref, sem).wait()
 
+    window = 2
     for g in range(groups):
+        if g > 0:
+            build_sel(g)
         out = jnp.dot(sel_v[g].reshape(rows, fold * tok), xn_v[...], preferred_element_type=F32)
         send_v[g] = out.astype(BF16).reshape(experts, mr, fw)
         if g == 0:
             pl.semaphore_wait(barrier, experts - 1 + tp - 1)
-        exchange(g, send_v, recv_v, dsend, drecv)
+        if g < window:
+            exchange(g, send_v, recv_v, dsend, drecv)
 
     own_row = chosen_v[pl.ds(me, 1), :].astype(F32)
 
@@ -190,6 +202,8 @@
 
     def gather_start(g):
         remote_wait(recv_v.at[g], drecv.at[g])
+        if g + window < groups:
+            exchange(g + window, send_v, recv_v, dsend, drecv)
         got = recv_v[g].reshape(rows, fw)
         piece_v[g, 0] = jnp.dot(pack_v[g], got, preferred_element_type=F32).astype(BF16)
         for r in range(1, chips):
@@ -381,9 +395,9 @@
 
 
 ORDER4 = [
-    "s1.0", "a.0", "s1.1", "s2.0", "m.0", "a.1", "b.0", "h.0", "s1.2", "s2.1", "x.0", "m.1", "a.2", "b.1", "h.1",
-    "s1.3", "s2.2", "x.1", "m.2", "l.0", "b.2", "h.2", "a.3", "x.2", "s2.3", "m.3", "l.1", "b.3", "h.3",
-    "x.3", "l.2", "r.0", "l.3", "r.1", "r.2", "r.3",
+    "s1.0", "s1.1", "a.0", "s2.0", "m.0", "b.0", "s1.2", "a.1", "h.0", "s2.1", "m.1", "x.0",
+    "s1.3", "b.1", "a.2", "s2.2", "h.1", "x.1", "m.2", "a.3", "b.2", "l.0", "h.2", "s2.3",
+    "m.3", "x.2", "b.3", "l.1", "h.3", "x.3", "l.2", "r.0", "l.3", "r.1", "r.2", "r.3",
 ]
 
 
@@ -440,7 +454,7 @@
         in_specs=[hbm] * 8,
         out_specs=pl.BlockSpec(memory_space=pltpu.VMEM),
         scratch_shapes=buffers + [
-            dma((4,)), dma((4,)), dma((3,)), dma((3,)), dma,
+            dma((2,)), dma((4,)), dma((3,)), dma((3,)), dma,
             dma, dma((groups,)), dma, dma((groups,)), dma, dma((groups, 2)),
             dma, dma((groups, 2)), dma, dma((groups,)), dma, dma((groups,)), dma, dma,
         ],

time: 46.3 us -> 45.7 us (0.987)
  Pallas kernels: 45.3 us -> 44.8 us
    pallas_call x1, Pallas kernels: 45.3 us -> 44.8 us  [on_device(): pl.pallas_call(functools.partial(layer, experts, tp, groups, fold, slots)...]
where the time goes in v3:
time: 45.7 us; the launch traced here: 45.5 us
  Pallas kernels  44.8 us (98%)
  local copies, waits for them, and re-layouts  0.75 us (2%)
    pallas_call x1, Pallas kernels, on_device(): pl.pallas_call(functools.partial(layer, experts, tp, groups, fold, slots)...  44.8 us

profile of v3, /device:TPU:0, one launch (start us, length us, event | category | flops | bytes accessed | tf_op | source)
XLA Modules:
  0.0 45.5 jit_solution(12999694820524281385)
XLA Ops:
  0.0 44.8 %layer.1 = bf16[256,768]{1,0:T(8,128)(2,1)S(1)} custom-call(bf16[256,3072]{1,0:T(8,128)(2,1)} %stream_hbm.1, bf16[24,128]{1,0:T(8,128)(2,1)} %bitcast.8, s32[8,256]{1,0:T(8,128)} %chosen_hbm.1, f32[1,256]{1,0:T(1,128)} %aff_hbm.1, bf16[3072,768]{1,0:T(8,128)(2,1)} %bitcast.5, bf16[3072,768]{1,0:T(8,128)(2,1)} %bitcast.6, bf16[768,3072]{1,0:T(8,128)(2,1)} %bitcast.7, ...), custom_call_target="tpu_custom_call" | custom-call | tf_op jit(solution)/shard_map/layer/pallas_call | solution.py:451
  44.8 0.7 %copy.10 = bf16[256,768]{1,0:T(8,128)(2,1)} copy(bf16[256,768]{1,0:T(8,128)(2,1)S(1)} %layer.1) | data formatting | bytes 786432

commit v4 on v3

--- a/solution.py
+++ b/solution.py
@@ -15,16 +15,16 @@
 
 
 def layer(
-    experts, tp, groups, fold, slots,
+    experts, tp, groups, fold, slots, full,
     stream_hbm, gain_hbm, chosen_hbm, aff_hbm, wg_hbm, wu_hbm, wd_hbm, fgain_hbm,
     out_ref,
-    x_v, xn_v, gain_v, gainf_v, chosen_v, aff_v, fgain_v, wg_v, wu_v, wd_v,
+    x_v, xn_v, xf_v, scale_v, gain_v, gainf_v, chosen_v, aff_v, fgain_v, wg_v, wu_v, wd_v,
     sel_v, place_v, pack_v, spread_v, affc_v,
-    send_v, recv_v, piece_v, accg_v, accu_v, hidden_v,
+    send_v, recv_v, sendf_v, recvf_v, piece_v, accg_v, accu_v, hidden_v,
     psend_v, pown_v, prec_v, ysend_v, yrec_v, leave_v, ret_v, merged_v, ssq_v,
     x_sem, s_sem, wg_sem, wu_sem, wd_sem,
     dsend, drecv, gsend, grecv, fsend, frecv, psend, precv, ysend, yrecv,
-    rsend, rrecv, qsend, qrecv,
+    rsend, rrecv, qsend, qrecv, hsend, hrecv,
 ):
     me = lax.axis_index("ep")
     col = lax.axis_index("tp")
@@ -97,9 +97,14 @@
     small[1].wait()
     gainf_v[...] = gain_v[...].astype(F32)
     lines = share // 128
-    gain = jnp.concatenate(
-        [gainf_v[pl.ds(partner * lines + i, 1), :] for i in range(lines)], axis=1
-    )
+
+    def gain_of(which):
+        return jnp.concatenate(
+            [gainf_v[pl.ds(which * lines + i, 1), :] for i in range(lines)], axis=1
+        )
+
+    opposite = (y + 1) % chips * 2 + 1 - core
+    gain = gain_of(partner)
     step = 32
     for i in range(pieces):
         x_copies[i].wait()
@@ -120,28 +125,34 @@
             at = pl.ds(i * xrows + b * step, step)
             block = x_v[at, :].astype(F32)
             scale = lax.rsqrt(jnp.sum(block * block, axis=1, keepdims=True) / width + EPSILON)
+            if full:
+                scale_v[at, :] = scale
             own = x_v[at, pl.ds(pl.multiple_of(partner * share, 128), share)].astype(F32)
             normed = (own * scale * gain).astype(BF16)
             for h in range(fold):
                 xn_v[pl.ds(h * tok + i * xrows + b * step, step), :] = normed[:, h * fw:(h + 1) * fw]
 
     far_first = sorted(range(experts), key=lambda r: -min(r, experts - r))
-    half_n = experts // 2
-    side = me // half_n
-
-    def target(i):
-        if i < half_n:
-            return (1 - side) * half_n + (me + i) % half_n
-        return side * half_n + (me + i + 1) % half_n
-
-    def exchange(g, src, dst, ssem, rsem):
-        for i in range(experts):
-            to = (me + far_first[i]) % experts
+    def exchange(g, src, dst, ssem, rsem, more=()):
+        for r in far_first:
+            to = (me + r) % experts
             pltpu.make_async_remote_copy(
                 src_ref=src.at[g, to], dst_ref=dst.at[g, me],
                 send_sem=ssem, recv_sem=rsem.at[g],
                 device_id={"ep": to, "tp": partner}, device_id_type=MESH,
             ).start()
+            for src_more, dst_more, ssem_more, rsem_more in more:
+                pltpu.make_async_remote_copy(
+                    src_ref=src_more.at[to], dst_ref=dst_more.at[me],
+                    send_sem=ssem_more, recv_sem=rsem_more,
+                    device_id={"ep": to, "tp": partner}, device_id_type=MESH,
+                ).start()
+
+    def dispatch(g):
+        both = full and g == groups - 1
+        exchange(
+            g, send_v, recv_v, dsend, drecv, [(sendf_v, recvf_v, hsend, hrecv)] if both else ()
+        )
 
     def remote_wait(ref, sem):
         pltpu.make_async_copy(ref, ref, sem).wait()
@@ -152,10 +163,20 @@
             build_sel(g)
         out = jnp.dot(sel_v[g].reshape(rows, fold * tok), xn_v[...], preferred_element_type=F32)
         send_v[g] = out.astype(BF16).reshape(experts, mr, fw)
+        if full and g == groups - 1:
+            gain_more = gain_of(opposite)
+            for b in range(tok // step):
+                at = pl.ds(b * step, step)
+                own = x_v[at, pl.ds(pl.multiple_of(opposite * share, 128), share)].astype(F32)
+                normed = (own * scale_v[at, :] * gain_more).astype(BF16)
+                for h in range(fold):
+                    xf_v[pl.ds(h * tok + b * step, step), :] = normed[:, h * fw:(h + 1) * fw]
+            out = jnp.dot(sel_v[g].reshape(rows, fold * tok), xf_v[...], preferred_element_type=F32)
+            sendf_v[...] = out.astype(BF16).reshape(experts, mr, fw)
         if g == 0:
             pl.semaphore_wait(barrier, experts - 1 + tp - 1)
         if g < window:
-            exchange(g, send_v, recv_v, dsend, drecv)
+            dispatch(g)
 
     own_row = chosen_v[pl.ds(me, 1), :].astype(F32)
 
@@ -203,9 +224,20 @@
     def gather_start(g):
         remote_wait(recv_v.at[g], drecv.at[g])
         if g + window < groups:
-            exchange(g + window, send_v, recv_v, dsend, drecv)
+            dispatch(g + window)
         got = recv_v[g].reshape(rows, fw)
         piece_v[g, 0] = jnp.dot(pack_v[g], got, preferred_element_type=F32).astype(BF16)
+        if full and g == groups - 1:
+            forward(g, 0)
+            remote_wait(recvf_v, hrecv)
+            got = recvf_v[...].reshape(rows, fw)
+            piece_v[g, 3] = jnp.dot(pack_v[g], got, preferred_element_type=F32).astype(BF16)
+            pltpu.make_async_remote_copy(
+                src_ref=piece_v.at[g, 3], dst_ref=piece_v.at[g, 2],
+                send_sem=fsend, recv_sem=frecv.at[g, 1],
+                device_id={"tp": partner}, device_id_type=MESH,
+            ).start()
+            return
         for r in range(1, chips):
             pltpu.make_async_remote_copy(
                 src_ref=piece_v.at[g, 0], dst_ref=piece_v.at[g, 2 * r],
@@ -258,8 +290,12 @@
         ]
 
     def near(g):
+        weight_wait(0)
+        if full and g == groups - 1:
+            weight_wait(2)
+            accg_v[g], accu_v[g] = contract(g, [0, 3])
+            return
         remote_wait(piece_v.at[g, 1], frecv.at[g, 0])
-        weight_wait(0)
         accg_v[g], accu_v[g] = contract(g, [0, 1])
 
     def middle(g):
@@ -270,8 +306,13 @@
 
     def away(g):
         remote_wait(piece_v.at[g, pl.ds(0, chips - 1)], frecv.at[g, 1])
-        weight_wait(2)
-        gate, up = contract(g, [2 * r + 1 for r in range(1, chips)])
+        if full and g == groups - 1:
+            remote_wait(piece_v.at[g, 1], frecv.at[g, 0])
+            weight_wait(1)
+            gate, up = contract(g, [1, 2])
+        else:
+            weight_wait(2)
+            gate, up = contract(g, [2 * r + 1 for r in range(1, chips)])
         gate = gate + accg_v[g]
         up = up + accu_v[g]
         hidden_v[g] = (gate / (1.0 + jnp.exp(-gate)) * up).astype(BF16)
@@ -386,7 +427,9 @@
 
     with jax.named_scope("fin"):
         remote_wait(send_v, dsend)
-        remote_wait(piece_v.at[:, pl.ds(0, chips - 1)], gsend)
+        if full:
+            remote_wait(sendf_v, hsend)
+        remote_wait(piece_v.at[pl.ds(0, groups - full), pl.ds(0, chips - 1)], gsend)
         remote_wait(piece_v.at[:, pl.ds(0, chips)], fsend)
         remote_wait(psend_v, psend)
         remote_wait(ysend_v.at[:, pl.ds(0, chips - 1)], ysend)
@@ -395,9 +438,9 @@
 
 
 ORDER4 = [
-    "s1.0", "s1.1", "a.0", "s2.0", "m.0", "b.0", "s1.2", "a.1", "h.0", "s2.1", "m.1", "x.0",
-    "s1.3", "b.1", "a.2", "s2.2", "h.1", "x.1", "m.2", "a.3", "b.2", "l.0", "h.2", "s2.3",
-    "m.3", "x.2", "b.3", "l.1", "h.3", "x.3", "l.2", "r.0", "l.3", "r.1", "r.2", "r.3",
+    "s1.0", "a.0", "s1.1", "s2.0", "m.0", "a.1", "b.0", "s1.2", "h.0", "s2.1", "x.0", "m.1",
+    "a.2", "b.1", "h.1", "s2.2", "x.1", "m.2", "b.2", "l.0", "s1.3", "h.2", "a.3", "x.2",
+    "l.1", "b.3", "h.3", "x.3", "l.2", "r.0", "l.3", "r.1", "r.2", "r.3",
 ]
 
 
@@ -414,11 +457,14 @@
     mr = slots // groups * fold
     rows = experts * mr
     chips = tp // 2
+    full = int(groups == 4 and chips == 2)
     hbm = pl.BlockSpec(memory_space=pltpu.HBM)
     dma = pltpu.SemaphoreType.DMA
     buffers = [
         pltpu.VMEM((tok, width), BF16),
         pltpu.VMEM((fold * tok, fw), BF16),
+        pltpu.VMEM((fold * tok, fw) if full else (8, 128), BF16),
+        pltpu.VMEM((tok, 1) if full else (8, 128), F32),
         pltpu.VMEM((width // 128, 128), BF16),
         pltpu.VMEM((width // 128, 128), F32),
         pltpu.VMEM((experts, caps), I32),
@@ -434,6 +480,8 @@
         pltpu.VMEM((groups, cg, 1), F32),
         pltpu.VMEM((groups, experts, mr, fw), BF16),
         pltpu.VMEM((groups, experts, mr, fw), BF16),
+        pltpu.VMEM((experts, mr, fw), BF16),
+        pltpu.VMEM((experts, mr, fw), BF16),
         pltpu.VMEM((groups, tp, fold * cg, fw), BF16),
         pltpu.VMEM((groups, cg, hid), F32),
         pltpu.VMEM((groups, cg, hid), F32),
@@ -449,14 +497,14 @@
         pltpu.VMEM((tp, 8, tok), F32),
     ]
     return pl.pallas_call(
-        functools.partial(layer, experts, tp, groups, fold, slots),
+        functools.partial(layer, experts, tp, groups, fold, slots, full),
         out_shape=pltpu.VMEM((tok, share), BF16),
         in_specs=[hbm] * 8,
         out_specs=pl.BlockSpec(memory_space=pltpu.VMEM),
         scratch_shapes=buffers + [
             dma((2,)), dma((4,)), dma((3,)), dma((3,)), dma,
             dma, dma((groups,)), dma, dma((groups,)), dma, dma((groups, 2)),
-            dma, dma((groups, 2)), dma, dma((groups,)), dma, dma((groups,)), dma, dma,
+            dma, dma((groups, 2)), dma, dma((groups,)), dma, dma((groups,)), dma, dma, dma, dma,
         ],
         compiler_params=pltpu.CompilerParams(
             collective_id=0, has_side_effects=True, vmem_limit_bytes=56 * 1024 * 1024

time: 45.7 us -> 45.3 us (level)
  Pallas kernels: 44.8 us -> 44.3 us
where the time goes in v4:
time: 45.3 us; the launch traced here: 45.1 us
  Pallas kernels  44.3 us (98%)
  local copies, waits for them, and re-layouts  0.75 us (2%)
    pallas_call x1, Pallas kernels, on_device(): pl.pallas_call(functools.partial(layer, experts, tp, groups, fold, slots,...  44.3 us

profile of v4, /device:TPU:0, one launch (start us, length us, event | category | flops | bytes accessed | tf_op | source)
XLA Modules:
  0.0 45.1 jit_solution(6340162884217732998)
XLA Ops:
  0.0 44.3 %layer.1 = bf16[256,768]{1,0:T(8,128)(2,1)S(1)} custom-call(bf16[256,3072]{1,0:T(8,128)(2,1)} %stream_hbm.1, bf16[24,128]{1,0:T(8,128)(2,1)} %bitcast.8, s32[8,256]{1,0:T(8,128)} %chosen_hbm.1, f32[1,256]{1,0:T(1,128)} %aff_hbm.1, bf16[3072,768]{1,0:T(8,128)(2,1)} %bitcast.5, bf16[3072,768]{1,0:T(8,128)(2,1)} %bitcast.6, bf16[768,3072]{1,0:T(8,128)(2,1)} %bitcast.7, ...), custom_call_target="tpu_custom_call" | custom-call | tf_op jit(solution)/shard_map/layer/pallas_call | solution.py:499
  44.3 0.7 %copy.10 = bf16[256,768]{1,0:T(8,128)(2,1)} copy(bf16[256,768]{1,0:T(8,128)(2,1)S(1)} %layer.1) | data formatting | bytes 786432

commit v5 on v4

--- a/solution.py
+++ b/solution.py
@@ -114,7 +114,7 @@
                     pltpu.make_async_copy(
                         src.at[pl.ds(frm * share, share), :],
                         dst.at[pl.ds(s * share, share), :],
-                        sem.at[0 if s < 2 else 1 + s % 2],
+                        sem,
                     ).start()
             for s, to in enumerate(scatter_cols):
                 pltpu.make_async_copy(
@@ -133,26 +133,20 @@
                 xn_v[pl.ds(h * tok + i * xrows + b * step, step), :] = normed[:, h * fw:(h + 1) * fw]
 
     far_first = sorted(range(experts), key=lambda r: -min(r, experts - r))
-    def exchange(g, src, dst, ssem, rsem, more=()):
+    def exchange(src, dst, ssem, rsem):
         for r in far_first:
             to = (me + r) % experts
             pltpu.make_async_remote_copy(
-                src_ref=src.at[g, to], dst_ref=dst.at[g, me],
-                send_sem=ssem, recv_sem=rsem.at[g],
+                src_ref=src.at[to], dst_ref=dst.at[me],
+                send_sem=ssem, recv_sem=rsem,
                 device_id={"ep": to, "tp": partner}, device_id_type=MESH,
             ).start()
-            for src_more, dst_more, ssem_more, rsem_more in more:
-                pltpu.make_async_remote_copy(
-                    src_ref=src_more.at[to], dst_ref=dst_more.at[me],
-                    send_sem=ssem_more, recv_sem=rsem_more,
-                    device_id={"ep": to, "tp": partner}, device_id_type=MESH,
-                ).start()
 
     def dispatch(g):
-        both = full and g == groups - 1
-        exchange(
-            g, send_v, recv_v, dsend, drecv, [(sendf_v, recvf_v, hsend, hrecv)] if both else ()
-        )
+        exchange(send_v.at[g], recv_v.at[g], dsend, drecv.at[g])
+
+    def dispatch_more(g):
+        exchange(sendf_v, recvf_v, hsend, hrecv)
 
     def remote_wait(ref, sem):
         pltpu.make_async_copy(ref, ref, sem).wait()
@@ -223,7 +217,7 @@
 
     def gather_start(g):
         remote_wait(recv_v.at[g], drecv.at[g])
-        if g + window < groups:
+        if window <= g + window < groups - full:
             dispatch(g + window)
         got = recv_v[g].reshape(rows, fw)
         piece_v[g, 0] = jnp.dot(pack_v[g], got, preferred_element_type=F32).astype(BF16)
@@ -263,12 +257,7 @@
     def weight_wait(n):
         if n not in waited:
             waited.add(n)
-            if n == 3:
-                remote_wait(wd_v, wd_sem)
-            else:
-                at = pl.ds(0, (2 if n == 0 else chips - 1) * share)
-                remote_wait(wg_v.at[at, :], wg_sem.at[n])
-                remote_wait(wu_v.at[at, :], wu_sem.at[n])
+            remote_wait((wg_v, wu_v, wd_v)[n], (wg_sem, wu_sem, wd_sem)[n])
 
     def contract(g, slots_in):
         taken = jnp.concatenate(
@@ -291,15 +280,14 @@
 
     def near(g):
         weight_wait(0)
+        weight_wait(1)
         if full and g == groups - 1:
-            weight_wait(2)
             accg_v[g], accu_v[g] = contract(g, [0, 3])
             return
         remote_wait(piece_v.at[g, 1], frecv.at[g, 0])
         accg_v[g], accu_v[g] = contract(g, [0, 1])
 
     def middle(g):
-        weight_wait(1)
         gate, up = contract(g, [2 * r for r in range(1, chips)])
         accg_v[g] += gate
         accu_v[g] += up
@@ -308,15 +296,13 @@
         remote_wait(piece_v.at[g, pl.ds(0, chips - 1)], frecv.at[g, 1])
         if full and g == groups - 1:
             remote_wait(piece_v.at[g, 1], frecv.at[g, 0])
-            weight_wait(1)
             gate, up = contract(g, [1, 2])
         else:
-            weight_wait(2)
             gate, up = contract(g, [2 * r + 1 for r in range(1, chips)])
         gate = gate + accg_v[g]
         up = up + accu_v[g]
         hidden_v[g] = (gate / (1.0 + jnp.exp(-gate)) * up).astype(BF16)
-        weight_wait(3)
+        weight_wait(2)
         for r in range(1, chips):
             pair(g, r)
 
@@ -357,7 +343,7 @@
         folded = jnp.concatenate([weighted[:, h * fw:(h + 1) * fw] for h in range(fold)], axis=0)
         out = jnp.dot(spread_v[g], folded, preferred_element_type=F32)
         leave_v[g] = out.astype(BF16).reshape(experts, mr, fw)
-        exchange(g, leave_v, ret_v, rsend, rrecv)
+        exchange(leave_v.at[g], ret_v.at[g], rsend, rrecv.at[g])
 
     def settle(g):
         remote_wait(ret_v.at[g], rrecv.at[g])
@@ -370,6 +356,7 @@
             merged_v[...] = merged_v[...] + update
 
     stages = {
+        "d": dispatch, "e": dispatch_more,
         "s1": gather_start, "s2": gather_forward, "a": near, "m": middle, "b": away, "h": home,
         "x": cross, "l": leave, "r": settle,
     }
@@ -396,7 +383,7 @@
         line = jnp.sum(
             jnp.where(eye, squares[b * square:(b + 1) * square, :], 0.0), axis=0, keepdims=True
         )
-        ssq_v[0, :, b * square:(b + 1) * square] = jnp.broadcast_to(line, (8, square))
+        ssq_v[0, :, b * square:(b + 1) * square] = line
 
     def square_copy(r):
         return pltpu.make_async_remote_copy(
@@ -438,9 +425,9 @@
 
 
 ORDER4 = [
-    "s1.0", "a.0", "s1.1", "s2.0", "m.0", "a.1", "b.0", "s1.2", "h.0", "s2.1", "x.0", "m.1",
-    "a.2", "b.1", "h.1", "s2.2", "x.1", "m.2", "b.2", "l.0", "s1.3", "h.2", "a.3", "x.2",
-    "l.1", "b.3", "h.3", "x.3", "l.2", "r.0", "l.3", "r.1", "r.2", "r.3",
+    "s1.0", "a.0", "s1.1", "d.3", "s2.0", "m.0", "a.1", "b.0", "e.3", "s1.2", "h.0", "s2.1",
+    "x.0", "m.1", "a.2", "b.1", "h.1", "s2.2", "x.1", "m.2", "b.2", "l.0", "s1.3", "h.2",
+    "a.3", "x.2", "l.1", "b.3", "h.3", "x.3", "l.2", "r.0", "l.3", "r.1", "r.2", "r.3",
 ]
 
 
@@ -494,7 +481,7 @@
         pltpu.VMEM((groups, experts, mr, fw), BF16),
         pltpu.VMEM((groups, experts, mr, fw), BF16),
         pltpu.VMEM((fold * tok, fw), F32),
-        pltpu.VMEM((tp, 8, tok), F32),
+        pltpu.VMEM((tp, 1, tok), F32),
     ]
     return pl.pallas_call(
         functools.partial(layer, experts, tp, groups, fold, slots, full),
@@ -502,7 +489,7 @@
         in_specs=[hbm] * 8,
         out_specs=pl.BlockSpec(memory_space=pltpu.VMEM),
         scratch_shapes=buffers + [
-            dma((2,)), dma((4,)), dma((3,)), dma((3,)), dma,
+            dma((2,)), dma((4,)), dma, dma, dma,
             dma, dma((groups,)), dma, dma((groups,)), dma, dma((groups, 2)),
             dma, dma((groups, 2)), dma, dma((groups,)), dma, dma((groups,)), dma, dma, dma, dma,
         ],

time: 45.3 us -> 44.8 us (0.989)
  Pallas kernels: 44.3 us -> 43.8 us
    pallas_call x1, Pallas kernels: 44.3 us -> 43.8 us  [on_device(): pl.pallas_call(functools.partial(layer, experts, tp, groups, fold, slots,...]
where the time goes in v5:
time: 44.8 us; the launch traced here: 44.6 us
  Pallas kernels  43.8 us (98%)
  local copies, waits for them, and re-layouts  0.75 us (2%)
    pallas_call x1, Pallas kernels, on_device(): pl.pallas_call(functools.partial(layer, experts, tp, groups, fold, slots,...  43.8 us

profile of v5, /device:TPU:0, one launch (start us, length us, event | category | flops | bytes accessed | tf_op | source)
XLA Modules:
  0.0 44.6 jit_solution(14600477453041539483)
XLA Ops:
  0.0 43.8 %layer.1 = bf16[256,768]{1,0:T(8,128)(2,1)S(1)} custom-call(bf16[256,3072]{1,0:T(8,128)(2,1)} %stream_hbm.1, bf16[24,128]{1,0:T(8,128)(2,1)} %bitcast.8, s32[8,256]{1,0:T(8,128)} %chosen_hbm.1, f32[1,256]{1,0:T(1,128)} %aff_hbm.1, bf16[3072,768]{1,0:T(8,128)(2,1)} %bitcast.5, bf16[3072,768]{1,0:T(8,128)(2,1)} %bitcast.6, bf16[768,3072]{1,0:T(8,128)(2,1)} %bitcast.7, ...), custom_call_target="tpu_custom_call" | custom-call | tf_op jit(solution)/shard_map/layer/pallas_call | solution.py:486
  43.8 0.7 %copy.10 = bf16[256,768]{1,0:T(8,128)(2,1)} copy(bf16[256,768]{1,0:T(8,128)(2,1)S(1)} %layer.1) | data formatting | bytes 786432

commit v6 on v5

--- a/solution.py
+++ b/solution.py
@@ -426,8 +426,8 @@
 
 ORDER4 = [
     "s1.0", "a.0", "s1.1", "d.3", "s2.0", "m.0", "a.1", "b.0", "e.3", "s1.2", "h.0", "s2.1",
-    "x.0", "m.1", "a.2", "b.1", "h.1", "s2.2", "x.1", "m.2", "b.2", "l.0", "s1.3", "h.2",
-    "a.3", "x.2", "l.1", "b.3", "h.3", "x.3", "l.2", "r.0", "l.3", "r.1", "r.2", "r.3",
+    "x.0", "m.1", "a.2", "b.1", "h.1", "s2.2", "x.1", "m.2", "s1.3", "b.2", "l.0", "h.2",
+    "a.3", "x.2", "b.3", "l.1", "h.3", "x.3", "l.2", "r.0", "l.3", "r.1", "r.2", "r.3",
 ]
 
 

time: 44.8 us -> 44.1 us (0.984)
  Pallas kernels: 43.8 us -> 43.1 us
    pallas_call x1, Pallas kernels: 43.8 us -> 43.1 us  [on_device(): pl.pallas_call(functools.partial(layer, experts, tp, groups, fold, slots,...]
where the time goes in v6:
time: 44.1 us; the launch traced here: 43.9 us
  Pallas kernels  43.1 us (98%)
  local copies, waits for them, and re-layouts  0.75 us (2%)
    pallas_call x1, Pallas kernels, on_device(): pl.pallas_call(functools.partial(layer, experts, tp, groups, fold, slots,...  43.1 us

profile of v6, /device:TPU:0, one launch (start us, length us, event | category | flops | bytes accessed | tf_op | source)
XLA Modules:
  0.0 43.9 jit_solution(11802914337824360058)
XLA Ops:
  0.0 43.1 %layer.1 = bf16[256,768]{1,0:T(8,128)(2,1)S(1)} custom-call(bf16[256,3072]{1,0:T(8,128)(2,1)} %stream_hbm.1, bf16[24,128]{1,0:T(8,128)(2,1)} %bitcast.8, s32[8,256]{1,0:T(8,128)} %chosen_hbm.1, f32[1,256]{1,0:T(1,128)} %aff_hbm.1, bf16[3072,768]{1,0:T(8,128)(2,1)} %bitcast.5, bf16[3072,768]{1,0:T(8,128)(2,1)} %bitcast.6, bf16[768,3072]{1,0:T(8,128)(2,1)} %bitcast.7, ...), custom_call_target="tpu_custom_call" | custom-call | tf_op jit(solution)/shard_map/layer/pallas_call | solution.py:486
  43.2 0.7 %copy.10 = bf16[256,768]{1,0:T(8,128)(2,1)} copy(bf16[256,768]{1,0:T(8,128)(2,1)S(1)} %layer.1) | data formatting | bytes 786432
